TPU v7x, 512 devices: a whole 4x4x16 slice. The times are simulated.
512 devices in a mesh: fs: 16 (over y, x), tp: 32 (over z, core).
Axes of the slice: x: 4, y: 4, z: 16, core: 2. Of those that a mesh axis runs over, the one named last changes fastest.
Arguments:
- value_input: bfloat16 [32768, 2048], P('fs', 'tp'), may hold values from -50 to 50
- value_cotangent: bfloat16 [32768, 512], P('fs'), may hold values from -6 to 6
- value_factor: bfloat16 [512, 128], replicated, may hold values from -10 to 10
- value_master: float32 [512, 2048], P('fs', 'tp'), may hold values from -0.125 to 0.125
- value_first: float32 [128, 2048], P('fs', 'tp'), may hold values from -4 to 4
- value_second: float32 [128, 2048], P('fs', 'tp'), may hold values from 0.01 to 0.2
- mixed_heads: bfloat16 [32768, 1024], P('fs', 'tp'), may hold values from -6 to 6
- output_cotangent: bfloat16 [32768, 2048], P('fs', 'tp'), may hold values from -50 to 50
- output_factor: bfloat16 [1024, 128], replicated, may hold values from -10 to 10
- output_master: float32 [1024, 2048], P('fs', 'tp'), may hold values from -0.1875 to 0.1875
- output_first: float32 [128, 2048], P('fs', 'tp'), may hold values from -4 to 4
- output_second: float32 [128, 2048], P('fs', 'tp'), may hold values from 0.01 to 0.2
Outputs:
- value_step: float32 [512, 2048], P('fs', 'tp')
- value_new_master: float32 [512, 2048], P('fs', 'tp')
- value_copy: bfloat16 [512, 2048], P(None, 'tp')
- value_first_new: float32 [128, 2048], P('fs', 'tp')
- value_second_new: float32 [128, 2048], P('fs', 'tp')
- output_step: float32 [1024, 2048], P('fs', 'tp')
- output_new_master: float32 [1024, 2048], P('fs', 'tp')
- output_copy: bfloat16 [1024, 2048], P(None, 'tp')
- output_first_new: float32 [128, 2048], P('fs', 'tp')
- output_second_new: float32 [128, 2048], P('fs', 'tp')
All inputs are finite; a program needn't handle non-finite values.
Results may differ from a plain program's by a relative error of at most 0.001.
Values may be sent and summed in bfloat16 or wider, within the bound.
A program may use at most 64 MiB of HBM per device.

v0:
```python
import jax
import jax.numpy as jnp
from jax import lax
from jax.sharding import Mesh
from jax.sharding import PartitionSpec as P

FS = ("fs_0", "fs_1")
TP = ("tp_0", "tp_1")
FS_TP = ("fs_0", "fs_1", "tp_0", "tp_1")
highest = lax.Precision.HIGHEST


def split_up(x, dim, count):
    dims = x.shape
    tiles = x.reshape(*dims[:dim], count, dims[dim] // count, *dims[dim + 1 :])
    return jnp.moveaxis(tiles, dim, 0)


def summed_on_arrival(x, axis, dim):
    count = lax.axis_size(axis)
    tiles = lax.all_to_all(split_up(x, dim, count), axis, 0, 0, tiled=True)
    return jnp.sum(tiles, axis=0)


def by_axis(x, axes):
    for axis in axes:
        x = lax.psum(x, axis)
    return x


def in_one_piece(arrays, axis, dim, along):
    both = jnp.concatenate(arrays, axis=along)
    whole, at, outs = (lax.all_gather(both, axis, axis=dim, tiled=True), 0, [])
    for a in arrays:
        outs.append(lax.slice_in_dim(whole, at, at + a.shape[along], axis=along))
        at += a.shape[along]
    return tuple(outs)


def joined_along(tiles, dim):
    dims = list(tiles.shape[1:])
    dims[dim] *= tiles.shape[0]
    return jnp.moveaxis(tiles, 0, dim).reshape(dims)


def gather_packed(arrays, axis, dims):
    flat = jnp.concatenate([a.reshape(-1) for a in arrays])
    lines, at, outs = (lax.all_gather(flat, axis), 0, [])
    for a, dim in zip(arrays, dims):
        tiles = lines[:, at : at + a.size].reshape(-1, *a.shape)
        outs.append(joined_along(tiles, dim))
        at += a.size
    return tuple(outs)


def tokens_exact(left, right):
    return lax.dot_general(
        left, right, (((0,), (0,)), ((), ())), precision=highest, preferred_element_type=jnp.float32
    )


def moment_update(projected, scale, first, second):
    scaled = scale * projected
    first_new = 0.9 * first + 0.1 * scaled
    second_new = 0.95 * second + 0.05 * scaled * scaled
    direction = first_new / (jnp.sqrt(second_new) + 1e-08)
    return (first_new, second_new, direction)


def project_both(value_image, output_image, value_input, output_cotangent, band):
    value_wide = value_input.astype(jnp.float32)
    output_wide = output_cotangent.astype(jnp.float32)
    columns = value_input.shape[1]
    blocks = 2 * band * lax.axis_size(FS) // (2 * band)
    value_term = tokens_exact(value_image, value_wide).reshape(blocks, band, columns)
    output_term = tokens_exact(output_image, output_wide).reshape(blocks, band, columns)
    paired = summed_on_arrival(
        jnp.stack([value_term, output_term], axis=1).reshape(2 * band * lax.axis_size(FS), columns),
        FS,
        0,
    )
    return (paired[:band], paired[band:])


def on_device(
    value_input,
    value_cotangent,
    value_factor,
    value_master,
    value_first,
    value_second,
    mixed_heads,
    output_cotangent,
    output_factor,
    output_master,
    output_first,
    output_second,
):
    fs_count = lax.axis_size(FS)
    fs_place = lax.axis_index(FS)
    rank = value_factor.shape[1]
    band = rank // fs_count
    columns = value_input.shape[1]
    value_rows = value_master.shape[0]
    output_rows = output_master.shape[0]
    value_block = lax.dynamic_slice_in_dim(
        value_factor, fs_place * value_rows, value_rows, 0
    ).astype(jnp.float32)
    output_block = lax.dynamic_slice_in_dim(
        output_factor, fs_place * output_rows, output_rows, 0
    ).astype(jnp.float32)
    value_image = jnp.dot(value_cotangent, value_factor, preferred_element_type=jnp.float32)
    heads_whole = lax.all_gather(mixed_heads, TP, axis=1, tiled=True)
    output_image = jnp.dot(heads_whole, output_factor, preferred_element_type=jnp.float32)
    value_proj, output_proj = project_both(
        value_image, output_image, value_input, output_cotangent, band
    )
    total_count = rank * columns * lax.axis_size(TP)
    value_square, output_square = (
        by_axis(jnp.sum(value_proj * value_proj), FS_TP),
        by_axis(jnp.sum(output_proj * output_proj), FS_TP),
    )
    value_scale = lax.rsqrt(value_square / total_count + 1e-06)
    output_scale = lax.rsqrt(output_square / total_count + 1e-06)
    value_first_new, value_second_new, value_dir = moment_update(
        value_proj, value_scale, value_first, value_second
    )
    output_first_new, output_second_new, output_dir = moment_update(
        output_proj, output_scale, output_first, output_second
    )
    value_dir_all, output_dir_all = in_one_piece((value_dir, output_dir), FS, 0, 1)
    value_step = jnp.dot(
        value_block, value_dir_all, precision=highest, preferred_element_type=jnp.float32
    )
    output_step = jnp.dot(
        output_block, output_dir_all, precision=highest, preferred_element_type=jnp.float32
    )
    value_new = value_master - 0.002 * value_step
    output_new = output_master - 0.002 * output_step
    value_copy, output_copy = gather_packed(
        (value_new.astype(jnp.bfloat16), output_new.astype(jnp.bfloat16)), FS, (0, 0)
    )
    return (
        value_step,
        value_new,
        value_copy,
        value_first_new,
        value_second_new,
        output_step,
        output_new,
        output_copy,
        output_first_new,
        output_second_new,
    )


def solution(mesh):
    split = Mesh(mesh.devices.reshape(4, 4, 16, 2), ("fs_0", "fs_1", "tp_0", "tp_1"))
    return jax.shard_map(
        on_device,
        mesh=split,
        in_specs=(
            P(FS, TP),
            P(FS, None),
            P(),
            P(FS, TP),
            P(FS, TP),
            P(FS, TP),
            P(FS, TP),
            P(FS, TP),
            P(),
            P(FS, TP),
            P(FS, TP),
            P(FS, TP),
        ),
        out_specs=(
            P(FS, TP),
            P(FS, TP),
            P(None, TP),
            P(FS, TP),
            P(FS, TP),
            P(FS, TP),
            P(FS, TP),
            P(None, TP),
            P(FS, TP),
            P(FS, TP),
        ),
        check_vma=False,
    )
```

profile of v0, /device:TPU:4, one launch (start us, length us, event | category | flops | bytes accessed | tf_op | source)
XLA Modules:
  0.0 218.8 jit_solution(8862395068048219859)
XLA Ops:
  7.2 0.0 copy-start
  7.2 0.0 copy-start.1
  7.2 0.0 all-gather.3.cloned.1.call-start
  7.2 0.7 all-gather.3.cloned.1.call-update
  7.9 0.8 copy-done
  8.8 1.6 fusion.14
  10.4 0.0 copy-start.2
  10.4 2.0 convolution_bitcast_fusion.1
  12.4 0.0 copy-start.5
  12.4 0.0 copy-start.6
  12.4 0.0 copy-start.7
  12.4 0.0 copy-start.8
  12.4 0.0 copy-start.3
  12.4 0.0 copy-start.4
  12.5 75.5 %all-gather.3.cloned.1.call-done = bf16[2048,1024]{0,1:T(8,128)(2,1)} async-done(((bf16[2048,32]{0,1:T(8,128)(2,1)}), bf16[2048,1024]{0,1:T(8,128)(2,1)}) %all-gather.3.cloned.1.call-update) | async-done | bytes 4194320 | tf_op jit(solution)/shard_map/all_gather | solution.py:113
  88.0 0.0 copy-done.1
  88.0 3.5 %fusion.15 = f32[2048,128]{1,0:T(8,128)S(1)} fusion(bf16[2048,1024]{0,1:T(8,128)(2,1)} %all-gather.3.cloned.1.call-done, bf16[1024,128]{1,0:T(8,128)(2,1)S(1)} %copy-done.1), kind=kOutput, calls=%fused_computation.31 | convolution fusion | flops 536870912 | bytes 5505024 | tf_op jit(solution)/shard_map/dot_general | solution.py:114
  91.4 0.0 copy-done.2
  91.5 1.0 convolution_bitcast_fusion
  92.5 0.8 reshape.29
  93.2 7.3 %all-to-all-start = ((f32[16,1,1024]{2,1,0:T(1,128)}), f32[16,1,1024]{2,1,0:T(1,128)S(1)}, u32[]{:S(2)}, u32[]{:S(2)}) async-start(f32[16,1,1024]{2,1,0:T(1,128)} %reshape.29), calls=%async_computation | async-start | bytes 131072 | tf_op jit(solution)/shard_map/all_to_all | solution.py:21
  100.5 5.5 %all-to-all-done = f32[16,1,1024]{2,1,0:T(1,128)S(1)} async-done(((f32[16,1,1024]{2,1,0:T(1,128)}), f32[16,1,1024]{2,1,0:T(1,128)S(1)}, u32[]{:S(2)}, u32[]{:S(2)}) %all-to-all-start) | async-done | bytes 65568 | tf_op jit(solution)/shard_map/all_to_all | solution.py:21
  106.0 0.5 broadcast.38
  106.6 0.8 reduce
  107.4 0.1 reshape.30
  107.5 0.6 multiply_reduce_fusion.1
  108.1 9.5 %all-reduce.2 = (f32[]{:T(128)}, f32[]{:T(128)}) all-reduce(f32[]{:T(128)} %get-tuple-element.31, f32[]{:T(128)} %get-tuple-element.30), channel_id=1, replica_groups=mesh['fs_0'=4,'fs_1'=4,'tp_0'=16,'tp_1'=2] {'fs_0'}, use_global_device_ids=true, to_apply=%region_7.0 | all-reduce | flops 2 | bytes 16 | tf_op jit(solution)/shard_map/psum | solution.py:27
  117.6 9.1 %all-reduce.1 = (f32[]{:T(128)}, f32[]{:T(128)}) all-reduce(f32[]{:T(128)} %get-tuple-element.36, f32[]{:T(128)} %get-tuple-element.37), channel_id=1, replica_groups=mesh['fs_0'=4,'fs_1'=4,'tp_0'=16,'tp_1'=2] {'fs_1'}, use_global_device_ids=true, to_apply=%region_8.0 | all-reduce | flops 2 | bytes 16 | tf_op jit(solution)/shard_map/psum | solution.py:27
  126.6 30.3 %all-reduce = (f32[]{:T(128)}, f32[]{:T(128)}) all-reduce(f32[]{:T(128)} %get-tuple-element.34, f32[]{:T(128)} %get-tuple-element.35), channel_id=1, replica_groups=mesh['fs_0'=4,'fs_1'=4,'tp_0'=16,'tp_1'=2] {'tp_0'}, use_global_device_ids=true, to_apply=%region_9.0 | all-reduce | flops 2 | bytes 16 | tf_op jit(solution)/shard_map/psum | solution.py:27
  156.9 3.1 %all-reduce.3 = (f32[]{:T(128)}, f32[]{:T(128)}) all-reduce(f32[]{:T(128)} %get-tuple-element.32, f32[]{:T(128)} %get-tuple-element.33), channel_id=1, replica_groups=mesh['fs_0'=4,'fs_1'=4,'tp_0'=16,'tp_1'=2] {'tp_1'}, use_global_device_ids=true, to_apply=%region_10.0 | all-reduce | flops 2 | bytes 16 | tf_op jit(solution)/shard_map/psum | solution.py:27
  161.4 0.0 copy-done.5
  161.4 0.0 copy-done.6
  161.4 0.0 copy-done.7
  161.4 0.0 copy-done.8
  161.4 0.6 add_divide_fusion.1
  162.0 0.1 pad_maximum_fusion.2
  162.1 22.1 %all_gather.13 = f32[128,128]{1,0:T(8,128)S(1)} all-gather(f32[8,128]{1,0:T(8,128)S(1)} %pad_maximum_fusion.2), channel_id=1, replica_groups=mesh['fs_0'=4,'fs_1'=4,'tp_0'=16,'tp_1'=2] {'fs_0','fs_1'}, dimensions={0}, use_global_device_ids=true | all-gather | bytes 69632 | tf_op jit(solution)/shard_map/all_gather | solution.py:33
  184.2 0.9 fusion.11
  185.1 0.1 reshape.27
  185.2 0.0 copy-done.4
  185.2 1.5 fusion.10
  186.6 0.1 reshape.26
  186.7 23.2 %all-gather = bf16[98304]{0:T(1024)(128)(2,1)S(1)} all-gather(bf16[6144]{0:T(1024)(128)(2,1)S(1)} %pad_maximum_fusion.1), channel_id=2, replica_groups=mesh['fs_0'=4,'fs_1'=4,'tp_0'=16,'tp_1'=2] {'fs_0','fs_1'}, dimensions={0}, use_global_device_ids=true | all-gather | bytes 208896 | tf_op jit(solution)/shard_map/all_gather | solution.py:48
  209.9 0.1 reshape.28
  210.0 0.2 reshape_reshape.11
  210.3 0.8 copy.31
  211.0 0.2 reshape_reshape.10
  211.2 0.7 copy.30
  (6 shorter events, 0.1 us)
Async XLA Ops:
  7.2 1.6 copy-start
  7.2 80.8 %copy-start.1 = (bf16[1024,128]{1,0:T(8,128)(2,1)S(1)}, bf16[1024,128]{1,0:T(8,128)(2,1)}, u32[]{:S(2)}) copy-start(bf16[1024,128]{1,0:T(8,128)(2,1)} %param.20) | copy-start | bytes 786436
  7.2 80.8 %all-gather.3.cloned.1.call-start = ((), (), s32[]{:S(2)}) async-start(), calls=%async_computation.1 | async-start | bytes 4325376 | tf_op jit(solution)/shard_map/all_gather | solution.py:113
  10.4 81.1 %copy-start.2 = (bf16[2048,64]{0,1:T(8,128)(2,1)S(1)}, bf16[2048,64]{0,1:T(8,128)(2,1)}, u32[]{:S(2)}) copy-start(bf16[2048,64]{0,1:T(8,128)(2,1)} %param.19) | copy-start | bytes 786436
  12.4 149.0 %copy-start.5 = (f32[8,64]{1,0:T(8,128)S(1)}, f32[8,64]{1,0:T(8,128)}, u32[]{:S(2)}) copy-start(f32[8,64]{1,0:T(8,128)} %param.17) | copy-start | bytes 6148
  12.4 149.0 %copy-start.6 = (f32[8,64]{1,0:T(8,128)S(1)}, f32[8,64]{1,0:T(8,128)}, u32[]{:S(2)}) copy-start(f32[8,64]{1,0:T(8,128)} %param.16) | copy-start | bytes 6148
  12.4 149.0 %copy-start.7 = (f32[8,64]{1,0:T(8,128)S(1)}, f32[8,64]{1,0:T(8,128)}, u32[]{:S(2)}) copy-start(f32[8,64]{1,0:T(8,128)} %param.23) | copy-start | bytes 6148
  12.4 149.0 %copy-start.8 = (f32[8,64]{1,0:T(8,128)S(1)}, f32[8,64]{1,0:T(8,128)}, u32[]{:S(2)}) copy-start(f32[8,64]{1,0:T(8,128)} %param.22) | copy-start | bytes 6148
  12.4 171.8 %copy-start.3 = (f32[64,64]{1,0:T(8,128)S(1)}, f32[64,64]{1,0:T(8,128)}, u32[]{:S(2)}) copy-start(f32[64,64]{1,0:T(8,128)} %param.21) | copy-start | bytes 49156
  12.4 172.7 %copy-start.4 = (f32[32,64]{1,0:T(8,128)S(1)}, f32[32,64]{1,0:T(8,128)}, u32[]{:S(2)}) copy-start(f32[32,64]{1,0:T(8,128)} %param.15) | copy-start | bytes 24580
  93.2 12.8 %all-to-all-start = ((f32[16,1,1024]{2,1,0:T(1,128)}), f32[16,1,1024]{2,1,0:T(1,128)S(1)}, u32[]{:S(2)}, u32[]{:S(2)}) async-start(f32[16,1,1024]{2,1,0:T(1,128)} %reshape.29), calls=%async_computation | async-start | bytes 131072 | tf_op jit(solution)/shard_map/all_to_all | solution.py:21
Sparse Core Ops, SparseCore 0:
  10.1 77.7 all-gather.2
where the time goes:
time: 219 us
  blocking collectives  97.2 us (44%)
  waiting for transfers between devices  81.7 us (37%)
  between operations  15.6 us (7%)
  matrix products  10.4 us (5%)
  starting transfers between devices  7.3 us (3%)
  local copies, waits for them, and re-layouts  4.46 us (2%)
    all_gather x1, waiting for transfers between devices, on_device(): heads_whole = lax.all_gather(mixed_heads, TP, axis=1, tiled=True)  75.5 us
    psum x4, blocking collectives, by_axis(): x = lax.psum(x, axis)  51.9 us
    all_gather x1, blocking collectives, gather_packed(): lines, at, outs = (lax.all_gather(flat, axis), 0, [])  23.2 us
    all_gather x1, blocking collectives, in_one_piece(): whole, at, outs = (lax.all_gather(both, axis, axis=dim, tiled=True), 0, [])  22.1 us
    all_to_all x1, starting transfers between devices, summed_on_arrival(): tiles = lax.all_to_all(split_up(x, dim, count), axis, 0, 0, tiled=True)  7.27 us
    all_to_all x1, waiting for transfers between devices, summed_on_arrival(): tiles = lax.all_to_all(split_up(x, dim, count), axis, 0, 0, tiled=True)  5.54 us
  transfers between devices with their start and end apart: 2, of which 2 were waited for; matrix products, arithmetic and copies ran while one was open for 2% of the time, Pallas kernels for 0%

commit v1 on v0

--- a/solution.py
+++ b/solution.py
@@ -110,7 +110,13 @@
         output_factor, fs_place * output_rows, output_rows, 0
     ).astype(jnp.float32)
     value_image = jnp.dot(value_cotangent, value_factor, preferred_element_type=jnp.float32)
-    heads_whole = lax.all_gather(mixed_heads, TP, axis=1, tiled=True)
+    unite_the_halves = lambda x_local, dev_axis: jnp.concatenate(
+        jax.lax.all_to_all(
+            jnp.stack([x_local for _ in range(jax.lax.axis_size(dev_axis))]), dev_axis, 0, 0
+        ),
+        axis=1,
+    )
+    heads_whole = unite_the_halves(mixed_heads, TP)
     output_image = jnp.dot(heads_whole, output_factor, preferred_element_type=jnp.float32)
     value_proj, output_proj = project_both(
         value_image, output_image, value_input, output_cotangent, band

time: 219 us -> 333 us (1.52)
  waiting for transfers between devices: 81.7 us -> 187 us
  starting transfers between devices: 7.3 us -> 23.2 us
  between operations: 15.6 us -> 2.23 us
  blocking collectives: 97.2 us -> 103 us
    all_to_all x0 -> x1, waiting for transfers between devices: none -> 182 us  [on_device(): jax.lax.all_to_all(jnp.stack([x_local for _ in range(jax.lax.axis_size(de...]
    all_gather x1 -> x0, waiting for transfers between devices: 75.5 us -> none  [on_device(): heads_whole = lax.all_gather(mixed_heads, TP, axis=1, tiled=True)]
    all_to_all x0 -> x1, starting transfers between devices: none -> 15.7 us  [on_device(): jax.lax.all_to_all(jnp.stack([x_local for _ in range(jax.lax.axis_size(de...]
    psum x4, blocking collectives: 51.9 us -> 57.3 us  [by_axis(): x = lax.psum(x, axis)]
    another operation x0 -> x1, local copies, waits for them, and re-layouts: none -> 3.54 us  [on_device(): jnp.stack([x_local for _ in range(jax.lax.axis_size(dev_axis))])]
  transfers between devices with their start and end apart: 2 -> 2, of which waited for: 2 -> 2; matrix products, arithmetic and copies ran while one was open for 2% -> 1% of each run, Pallas kernels for 0% -> 0%
where the time goes in v1:
time: 333 us; the launch traced here: 332 us
  waiting for transfers between devices  187 us (56%)
  blocking collectives  103 us (31%)
  starting transfers between devices  23.2 us (7%)
  matrix products  7.85 us (2%)
  local copies, waits for them, and re-layouts  7.17 us (2%)
    all_to_all x1, waiting for transfers between devices, on_device(): jax.lax.all_to_all(jnp.stack([x_local for _ in range(jax.lax.axis_size(de...  182 us
    psum x4, blocking collectives, by_axis(): x = lax.psum(x, axis)  57.3 us
    all_gather x1, blocking collectives, gather_packed(): lines, at, outs = (lax.all_gather(flat, axis), 0, [])  23.2 us
    all_gather x1, blocking collectives, in_one_piece(): whole, at, outs = (lax.all_gather(both, axis, axis=dim, tiled=True), 0, [])  22.1 us
    all_to_all x1, starting transfers between devices, on_device(): jax.lax.all_to_all(jnp.stack([x_local for _ in range(jax.lax.axis_size(de...  15.7 us
    all_to_all x1, starting transfers between devices, summed_on_arrival(): tiles = lax.all_to_all(split_up(x, dim, count), axis, 0, 0, tiled=True)  7.45 us
  transfers between devices with their start and end apart: 2, of which 2 were waited for; matrix products, arithmetic and copies ran while one was open for 1% of the time, Pallas kernels for 0%

profile of v1, /device:TPU:4, one launch (start us, length us, event | category | flops | bytes accessed | tf_op | source)
XLA Modules:
  0.0 332.4 jit_solution(14355748823505048202)
XLA Ops:
  0.6 0.0 copy-start
  0.7 3.5 %stack.4 = bf16[32,2048,32]{1,2,0:T(8,128)(2,1)} broadcast(bf16[2048,32]{0,1:T(8,128)(2,1)} %param.18), dimensions={1,2} | broadcast | bytes 4325376 | tf_op jit(solution)/shard_map/stack | solution.py:115
  4.2 15.7 %all-to-all-start = ((bf16[32,2048,32]{1,2,0:T(8,128)(2,1)}), bf16[32,2048,32]{1,2,0:T(8,128)(2,1)}, u32[]{:S(2)}, u32[]{:S(2)}) async-start(bf16[32,2048,32]{1,2,0:T(8,128)(2,1)} %stack.4), calls=%async_computation | async-start | bytes 8388608 | tf_op jit(solution)/shard_map/all_to_all | solution.py:114
  20.0 0.0 copy-done
  20.0 0.0 copy-done.4
  20.0 0.0 copy-start.1
  20.0 0.7 fusion.14
  20.7 0.0 copy-done.2
  20.7 0.0 copy-start.3
  20.7 1.0 convolution_bitcast_fusion.1
  21.7 181.7 %all-to-all-done = bf16[32,2048,32]{1,2,0:T(8,128)(2,1)} async-done(((bf16[32,2048,32]{1,2,0:T(8,128)(2,1)}), bf16[32,2048,32]{1,2,0:T(8,128)(2,1)}, u32[]{:S(2)}, u32[]{:S(2)}) %all-to-all-start) | async-done | bytes 4194336 | tf_op jit(solution)/shard_map/all_to_all | solution.py:114
  203.5 0.0 copy-done.1
  203.5 0.0 copy-start.10
  203.5 0.0 copy-start.5
  203.5 0.0 copy-start.6
  203.5 3.5 %fusion.15 = f32[2048,128]{1,0:T(8,128)S(1)} fusion(bf16[2048,1024]{0,1:T(8,128)(2,1)} %bitcast.2, bf16[1024,128]{1,0:T(8,128)(2,1)S(1)} %copy-done.1), kind=kOutput, calls=%fused_computation.31 | convolution fusion | flops 536870912 | bytes 5505024 | tf_op jit(solution)/shard_map/dot_general | solution.py:120
  207.0 0.0 copy-done.3
  207.0 1.0 convolution_bitcast_fusion
  208.1 0.8 reshape.39
  208.8 7.4 %all-to-all-start.1 = ((f32[16,1,1024]{2,1,0:T(1,128)}), f32[16,1,1024]{2,1,0:T(1,128)S(1)}, u32[]{:S(2)}, u32[]{:S(2)}) async-start(f32[16,1,1024]{2,1,0:T(1,128)} %reshape.39), calls=%async_computation.1 | async-start | bytes 131072 | tf_op jit(solution)/shard_map/all_to_all | solution.py:21
  216.3 5.5 %all-to-all-done.1 = f32[16,1,1024]{2,1,0:T(1,128)S(1)} async-done(((f32[16,1,1024]{2,1,0:T(1,128)}), f32[16,1,1024]{2,1,0:T(1,128)S(1)}, u32[]{:S(2)}, u32[]{:S(2)}) %all-to-all-start.1) | async-done | bytes 65568 | tf_op jit(solution)/shard_map/all_to_all | solution.py:21
  221.8 0.5 broadcast.40
  222.3 0.8 reduce
  223.1 0.1 reshape.40
  223.2 0.6 multiply_reduce_fusion.1
  223.9 9.5 %all-reduce.2 = (f32[]{:T(128)}, f32[]{:T(128)}) all-reduce(f32[]{:T(128)} %get-tuple-element.31, f32[]{:T(128)} %get-tuple-element.30), channel_id=1, replica_groups=mesh['fs_0'=4,'fs_1'=4,'tp_0'=16,'tp_1'=2] {'fs_0'}, use_global_device_ids=true, to_apply=%region_7.0 | all-reduce | flops 2 | bytes 16 | tf_op jit(solution)/shard_map/psum | solution.py:27
  233.4 9.1 %all-reduce.1 = (f32[]{:T(128)}, f32[]{:T(128)}) all-reduce(f32[]{:T(128)} %get-tuple-element.36, f32[]{:T(128)} %get-tuple-element.37), channel_id=1, replica_groups=mesh['fs_0'=4,'fs_1'=4,'tp_0'=16,'tp_1'=2] {'fs_1'}, use_global_device_ids=true, to_apply=%region_8.0 | all-reduce | flops 2 | bytes 16 | tf_op jit(solution)/shard_map/psum | solution.py:27
  242.4 35.6 %all-reduce = (f32[]{:T(128)}, f32[]{:T(128)}) all-reduce(f32[]{:T(128)} %get-tuple-element.34, f32[]{:T(128)} %get-tuple-element.35), channel_id=1, replica_groups=mesh['fs_0'=4,'fs_1'=4,'tp_0'=16,'tp_1'=2] {'tp_0'}, use_global_device_ids=true, to_apply=%region_9.0 | all-reduce | flops 2 | bytes 16 | tf_op jit(solution)/shard_map/psum | solution.py:27
  278.0 3.1 all-reduce.3
  282.5 0.0 copy-done.7
  282.5 0.0 copy-done.8
  282.5 0.0 copy-done.9
  282.5 0.0 copy-done.10
  282.5 0.6 add_divide_fusion.1
  283.1 0.1 pad_maximum_fusion.2
  283.2 22.1 %all_gather.9 = f32[128,128]{1,0:T(8,128)S(1)} all-gather(f32[8,128]{1,0:T(8,128)S(1)} %pad_maximum_fusion.2), channel_id=1, replica_groups=mesh['fs_0'=4,'fs_1'=4,'tp_0'=16,'tp_1'=2] {'fs_0','fs_1'}, dimensions={0}, use_global_device_ids=true | all-gather | bytes 69632 | tf_op jit(solution)/shard_map/all_gather | solution.py:33
  305.3 0.0 copy-done.5
  305.3 0.9 fusion.11
  306.2 0.1 reshape.37
  306.3 0.0 copy-done.6
  306.3 0.8 fusion.10
  307.1 0.1 reshape.36
  307.2 23.2 %all-gather = bf16[98304]{0:T(1024)(128)(2,1)S(1)} all-gather(bf16[6144]{0:T(1024)(128)(2,1)S(1)} %pad_maximum_fusion.1), channel_id=2, replica_groups=mesh['fs_0'=4,'fs_1'=4,'tp_0'=16,'tp_1'=2] {'fs_0','fs_1'}, dimensions={0}, use_global_device_ids=true | all-gather | bytes 208896 | tf_op jit(solution)/shard_map/all_gather | solution.py:48
  330.3 0.1 reshape.38
  330.4 0.2 reshape_reshape.11
  330.7 0.8 copy.32
  331.5 0.2 reshape_reshape.10
  331.6 0.7 copy.31
  (10 shorter events, 0.1 us)
Async XLA Ops:
  0.6 19.3 %copy-start = (bf16[2048,512]{1,0:T(8,128)(2,1)S(1)}, bf16[2048,512]{1,0:T(8,128)(2,1)}, u32[]{:S(2)}) copy-start(bf16[2048,512]{1,0:T(8,128)(2,1)} %param.13) | copy-start | bytes 6291460
  4.2 15.8 %copy-start.4 = (bf16[512,128]{1,0:T(8,128)(2,1)S(1)}, bf16[512,128]{1,0:T(8,128)(2,1)}, u32[]{:S(2)}) copy-start(bf16[512,128]{1,0:T(8,128)(2,1)} %param.14) | copy-start | bytes 393220
  4.2 16.5 %copy-start.2 = (bf16[2048,64]{0,1:T(8,128)(2,1)S(1)}, bf16[2048,64]{0,1:T(8,128)(2,1)}, u32[]{:S(2)}) copy-start(bf16[2048,64]{0,1:T(8,128)(2,1)} %param.12) | copy-start | bytes 786436
  4.2 199.2 %all-to-all-start = ((bf16[32,2048,32]{1,2,0:T(8,128)(2,1)}), bf16[32,2048,32]{1,2,0:T(8,128)(2,1)}, u32[]{:S(2)}, u32[]{:S(2)}) async-start(bf16[32,2048,32]{1,2,0:T(8,128)(2,1)} %stack.4), calls=%async_computation | async-start | bytes 8388608 | tf_op jit(solution)/shard_map/all_to_all | solution.py:114
  20.0 183.5 %copy-start.1 = (bf16[1024,128]{1,0:T(8,128)(2,1)S(1)}, bf16[1024,128]{1,0:T(8,128)(2,1)}, u32[]{:S(2)}) copy-start(bf16[1024,128]{1,0:T(8,128)(2,1)} %param.20) | copy-start | bytes 786436
  20.7 186.3 %copy-start.3 = (bf16[2048,64]{0,1:T(8,128)(2,1)S(1)}, bf16[2048,64]{0,1:T(8,128)(2,1)}, u32[]{:S(2)}) copy-start(bf16[2048,64]{0,1:T(8,128)(2,1)} %param.19) | copy-start | bytes 786436
  203.5 79.0 %copy-start.7 = (f32[8,64]{1,0:T(8,128)S(1)}, f32[8,64]{1,0:T(8,128)}, u32[]{:S(2)}) copy-start(f32[8,64]{1,0:T(8,128)} %param.17) | copy-start | bytes 6148
  203.5 79.0 %copy-start.8 = (f32[8,64]{1,0:T(8,128)S(1)}, f32[8,64]{1,0:T(8,128)}, u32[]{:S(2)}) copy-start(f32[8,64]{1,0:T(8,128)} %param.16) | copy-start | bytes 6148
  203.5 79.1 %copy-start.9 = (f32[8,64]{1,0:T(8,128)S(1)}, f32[8,64]{1,0:T(8,128)}, u32[]{:S(2)}) copy-start(f32[8,64]{1,0:T(8,128)} %param.23) | copy-start | bytes 6148
  203.5 79.1 %copy-start.10 = (f32[8,64]{1,0:T(8,128)S(1)}, f32[8,64]{1,0:T(8,128)}, u32[]{:S(2)}) copy-start(f32[8,64]{1,0:T(8,128)} %param.22) | copy-start | bytes 6148
  203.5 101.9 %copy-start.5 = (f32[64,64]{1,0:T(8,128)S(1)}, f32[64,64]{1,0:T(8,128)}, u32[]{:S(2)}) copy-start(f32[64,64]{1,0:T(8,128)} %param.21) | copy-start | bytes 49156
  203.5 102.8 %copy-start.6 = (f32[32,64]{1,0:T(8,128)S(1)}, f32[32,64]{1,0:T(8,128)}, u32[]{:S(2)}) copy-start(f32[32,64]{1,0:T(8,128)} %param.15) | copy-start | bytes 24580
  208.8 13.0 %all-to-all-start.1 = ((f32[16,1,1024]{2,1,0:T(1,128)}), f32[16,1,1024]{2,1,0:T(1,128)S(1)}, u32[]{:S(2)}, u32[]{:S(2)}) async-start(f32[16,1,1024]{2,1,0:T(1,128)} %reshape.39), calls=%async_computation.1 | async-start | bytes 131072 | tf_op jit(solution)/shard_map/all_to_all | solution.py:21
